TPU v7x, 32 devices: a whole 2x2x4 slice. The times are simulated.
32 devices in a mesh: grp: 2 (over x), tp: 4 (over z), dp: 4 (over y, core).
Axes of the slice: x: 2, y: 2, z: 4, core: 2. Of those that a mesh axis runs over, the one named last changes fastest.
Arguments:
- stream: bfloat16 [32, 4096], P('grp', 'dp'), parts along dimension 0, may hold values from -11 to 11
- states: float32 [2, 32, 32, 64, 64], P(None, ('grp', 'dp'), 'tp'), parts along dimension 1, may hold values from -6 to 6
- norm_gain: bfloat16 [2, 4096], P(None, 'dp'), may hold values from 0.099609375 to 1.8984375
- recept_weight: bfloat16 [2, 4096, 2048], P(None, 'dp', 'tp'), may hold values from -0.09375 to 0.09375
- key_weight: bfloat16 [2, 4096, 2048], P(None, 'dp', 'tp'), may hold values from -0.09375 to 0.09375
- value_weight: bfloat16 [2, 4096, 2048], P(None, 'dp', 'tp'), may hold values from -0.09375 to 0.09375
- decay_weight: bfloat16 [2, 4096, 2048], P(None, 'dp', 'tp'), may hold values from -0.09375 to 0.09375
- rate_weight: bfloat16 [2, 4096, 2048], P(None, 'dp', 'tp'), may hold values from -0.09375 to 0.09375
- gate_weight: bfloat16 [2, 4096, 2048], P(None, 'dp', 'tp'), may hold values from -0.09375 to 0.09375
- out_weight: bfloat16 [2, 2048, 4096], P(None, 'tp', 'dp'), may hold values from -0.125 to 0.125
- decay_bias: float32 [2, 2048], P(None, 'tp'), may hold values from -2 to 2
- head_gain: bfloat16 [2, 2048], P(None, 'tp'), may hold values from 0.099609375 to 1.8984375
Outputs:
- new_stream: bfloat16 [32, 4096], P('grp', 'dp'), parts along dimension 0
- new_states: float32 [2, 32, 32, 64, 64], P(None, ('grp', 'dp'), 'tp'), parts along dimension 1
There are 2 independent parts, one for each index of `grp`. A program takes and returns all parts, laid end to end along the dimension named above; an argument that names none is the same for every part. Nothing has to cross between parts.
All inputs are finite; a program needn't handle non-finite values.
Results may differ from a plain program's by a relative error of at most 0.0068.
Values may be sent and summed in bfloat16 or wider, within the bound.
A program may use at most 64 MiB of HBM per device.

v0:
```python
import jax
import jax.numpy as jnp
from jax import lax
from jax.sharding import PartitionSpec as P

D = 4096
HEAD = 64


def run_block(stream, state_blk, gain, weights, out_weight, bias, hgain):
    current = stream.astype(jnp.float32)
    squares = jnp.sum(current * current, axis=1)
    normed = (current * gain.astype(jnp.float32)).astype(jnp.bfloat16)
    width = weights[0].shape[1]
    local_rows = state_blk.shape[0]
    all_totals = lax.psum(squares, "dp")
    offset = lax.axis_index("dp") * local_rows
    totals = lax.dynamic_slice_in_dim(all_totals, offset, local_rows, 0)
    summed = lax.psum_scatter(
        jnp.concatenate(
            [jnp.dot(normed, weight, preferred_element_type=jnp.float32) for weight in weights],
            axis=1,
        ),
        "dp",
        scatter_dimension=0,
        tiled=True,
    )
    inv_rms = lax.rsqrt(totals / D + 1e-06)[:, None]
    projected = (summed * inv_rms).reshape(local_rows, 6, -1, HEAD)
    recept = projected[:, 0]
    key_vec = projected[:, 1]
    value_vec = projected[:, 2]
    decay_pre = projected[:, 3]
    rate_pre = projected[:, 4]
    gate_pre = projected[:, 5]
    unit_key = key_vec * lax.rsqrt(jnp.sum(key_vec * key_vec, axis=2, keepdims=True) + 1e-06)
    rate_vec = jax.nn.sigmoid(rate_pre)
    decay = jnp.exp(-0.606531 * jax.nn.sigmoid(bias.reshape(1, -1, HEAD) + decay_pre))
    removed = jnp.einsum("bhij,bhj->bhi", state_blk, unit_key, precision=lax.Precision.HIGHEST)
    new_state = (
        state_blk * decay[:, :, None, :]
        - removed[..., None] * (unit_key * rate_vec)[:, :, None, :]
        + value_vec[..., None] * key_vec[:, :, None, :]
    )
    read = jnp.einsum("bhij,bhj->bhi", new_state, recept, precision=lax.Precision.HIGHEST)
    center = read - jnp.mean(read, axis=2, keepdims=True)
    normal_read = center * lax.rsqrt(jnp.mean(center * center, axis=2, keepdims=True) + 1e-05)
    gated = normal_read * hgain.astype(jnp.float32).reshape(1, -1, HEAD) * jax.nn.sigmoid(gate_pre)
    mixed = gated.reshape(local_rows, width).astype(jnp.bfloat16)
    branch_part = jnp.dot(
        lax.all_gather(mixed, "dp", axis=0, tiled=True),
        out_weight,
        preferred_element_type=jnp.float32,
    )
    branch = lax.psum(branch_part, "tp")
    return ((current + branch).astype(jnp.bfloat16), new_state)


def per_device(
    stream,
    states,
    norm_gain,
    recept_weight,
    key_weight,
    value_weight,
    decay_weight,
    rate_weight,
    gate_weight,
    out_weight,
    decay_bias,
    head_gain,
):
    current = stream
    fresh_list = []
    for layer in range(2):
        weights = (
            recept_weight[layer],
            key_weight[layer],
            value_weight[layer],
            decay_weight[layer],
            rate_weight[layer],
            gate_weight[layer],
        )
        current, fresh = run_block(
            current,
            states[layer],
            norm_gain[layer],
            weights,
            out_weight[layer],
            decay_bias[layer],
            head_gain[layer],
        )
        fresh_list.append(fresh)
    return (current, jnp.stack(fresh_list))


def solution(mesh):
    in_specs = (
        P("grp", "dp"),
        P(None, ("grp", "dp"), "tp", None, None),
        P(None, "dp"),
        P(None, "dp", "tp"),
        P(None, "dp", "tp"),
        P(None, "dp", "tp"),
        P(None, "dp", "tp"),
        P(None, "dp", "tp"),
        P(None, "dp", "tp"),
        P(None, "tp", "dp"),
        P(None, "tp"),
        P(None, "tp"),
    )
    out_specs = (P("grp", "dp"), P(None, ("grp", "dp"), "tp", None, None))
    return jax.shard_map(
        per_device, mesh=mesh, in_specs=in_specs, out_specs=out_specs, check_vma=False
    )
```

profile of v0, /device:TPU:0, one launch (start us, length us, event | category | flops | bytes accessed | tf_op | source)
XLA Modules:
  0.0 201.3 jit_solution(15151777179491624203)
XLA Ops:
  7.2 0.9 slice_convert_fusion
  8.1 1.6 convolution_dynamic-update-slice_fusion.11
  9.7 1.5 convolution_dynamic-update-slice_fusion.10
  11.5 1.6 convolution_dynamic-update-slice_fusion.8
  13.4 1.5 convolution_dynamic-update-slice_fusion.6
  14.9 0.7 copy-done.6
  15.8 8.4 %psum.28 = f32[16]{0:T(128)S(1)} all-reduce(f32[16]{0:T(128)S(1)} %fusion.61), channel_id=1, replica_groups=mesh['grp'=2,'tp'=4,'dp'=4] {'dp'}, use_global_device_ids=true, to_apply=%region_2.0 | all-reduce | flops 16 | bytes 128 | tf_op jit(solution)/shard_map/psum | solution.py:16
  24.4 0.6 dynamic-slice
  25.7 24.8 %all-reduce.11.cloned.1.call-done = f32[16,3072]{1,0:T(8,128)} async-done(((f32[16,3072]{1,0:T(8,128)}), f32[16,3072]{1,0:T(8,128)}) %all-reduce.11.cloned.1.call-update) | async-done | bytes 196624
  50.5 1.0 dynamic-slice_multiply_fusion.1
  51.7 1.7 fusion.22
  53.5 2.1 %fusion.26 = f32[4,8,1,64]{3,2,1,0:T(1,128)S(1)} fusion(f32[4,8,64,1]{2,3,1,0:T(1,128)S(1)} %bitcast.192, f32[2,4,8,64,64]{4,3,2,1,0:T(8,128)S(1)} %copy-done, f32[4,8,64]{2,1,0:T(8,128)S(1)} %get-tuple-element.23, f32[4,8,64]{2,1,0:T(8,128)S(1)} %get-tuple-element.21, f32[4,8,64]{2,1,0:T(8,128)S(1)} %get-tuple-element.10, f32[4,8,64]{2,1,0:T(8,128)S(1)} %bitcast.185, ...), kind=kOutput, calls=%fused_computation.40 | convolution fusion | flops 2228224 | bytes 1155072 | tf_op jit(solution)/shard_map/bhij,bhj->bhi/dot_general | solution.py:45
  56.0 5.2 %all-gather = bf16[4,4,512]{2,1,0:T(4,128)(2,1)S(1)} all-gather(bf16[1,4,512]{2,1,0:T(4,128)(2,1)S(1)} %reshape.168), channel_id=1, replica_groups=mesh['grp'=2,'tp'=4,'dp'=4] {'dp'}, dimensions={0}, use_global_device_ids=true | all-gather | bytes 20480 | tf_op jit(solution)/shard_map/all_gather | solution.py:51
  61.2 2.1 %fusion.14 = f32[16,1024]{1,0:T(8,128)} fusion(bf16[16,512]{1,0:T(8,128)(2,1)S(1)} %reshape.169, bf16[2,512,1024]{2,1,0:T(8,128)(2,1)} %param.21), kind=kOutput, calls=%fused_computation.27 | convolution fusion | flops 16777216 | bytes 1130496 | tf_op jit(solution)/shard_map/dot_general | solution.py:50
  63.5 34.3 %all-reduce.7.cloned.1.call-done = f32[16,1024]{1,0:T(8,128)} async-done(((f32[16,1024]{1,0:T(8,128)}), f32[16,1024]{1,0:T(8,128)}) %all-reduce.7.cloned.1.call-update) | async-done | bytes 65552 | tf_op jit(solution)/shard_map/psum | solution.py:55
  97.8 1.0 fusion.64
  98.8 5.7 %psum.30 = f32[16]{0:T(128)S(1)} all-reduce(f32[16]{0:T(128)S(1)} %get-tuple-element.8), channel_id=1, replica_groups=mesh['grp'=2,'tp'=4,'dp'=4] {'dp'}, use_global_device_ids=true, to_apply=%region_9.0 | all-reduce | flops 16 | bytes 128 | tf_op jit(solution)/shard_map/psum | solution.py:16
  104.4 1.6 convolution_dynamic-update-slice_fusion.5
  106.1 1.5 convolution_dynamic-update-slice_fusion.4
  107.8 1.5 convolution_dynamic-update-slice_fusion.2
  109.5 1.5 convolution_dynamic-update-slice_fusion
  111.0 0.7 copy-done.7
  111.8 32.0 %all-reduce.13.cloned.1.call-done = f32[16,3072]{1,0:T(8,128)} async-done(((f32[16,3072]{1,0:T(8,128)}), f32[16,3072]{1,0:T(8,128)}) %all-reduce.13.cloned.1.call-update) | async-done | bytes 196624
  143.8 1.0 dynamic-slice_multiply_fusion
  145.1 1.7 fusion.8
  146.8 2.2 %multiply_add_fusion.1 = (f32[1,4,8,64,64]{4,3,2,1,0:T(8,128)S(1)}, f32[1,4,8,64,64]{4,3,2,1,0:T(8,128)}) fusion(f32[2,4,8,64,64]{4,3,2,1,0:T(8,128)S(1)} %copy-done, f32[4,8,64]{2,1,0:T(8,128)S(1)} %get-tuple-element.23, f32[4,8,64]{2,1,0:T(8,128)S(1)} %get-tuple-element.21, f32[4,8,64]{2,1,0:T(8,128)S(1)} %get-tuple-element.10, ...), kind=kLoop, calls=%fused_computation.42 | loop fusion | flops 1310720 | bytes 2179072 | tf_op jit(solution)/shard_map/add | solution.py:41
  149.0 2.1 %fusion.12 = f32[4,8,1,64]{3,2,1,0:T(1,128)S(1)} fusion(f32[4,8,64,1]{2,3,1,0:T(1,128)S(1)} %bitcast.191, f32[2,4,8,64,64]{4,3,2,1,0:T(8,128)S(1)} %copy-done, f32[4,8,64]{2,1,0:T(8,128)S(1)} %get-tuple-element.18, f32[4,8,64]{2,1,0:T(8,128)S(1)} %get-tuple-element.16, f32[4,8,64]{2,1,0:T(8,128)S(1)} %get-tuple-element.6, f32[4,8,64]{2,1,0:T(8,128)S(1)} %bitcast.188, ...), kind=kOutput, calls=%fused_computation.26 | convolution fusion | flops 2228224 | bytes 1155072 | tf_op jit(solution)/shard_map/bhij,bhj->bhi/dot_general | solution.py:45
  151.5 5.2 %all-gather.1 = bf16[4,4,512]{2,1,0:T(4,128)(2,1)S(1)} all-gather(bf16[1,4,512]{2,1,0:T(4,128)(2,1)S(1)} %reshape.170), channel_id=1, replica_groups=mesh['grp'=2,'tp'=4,'dp'=4] {'dp'}, dimensions={0}, use_global_device_ids=true | all-gather | bytes 20480 | tf_op jit(solution)/shard_map/all_gather | solution.py:51
  156.8 2.1 %fusion = f32[16,1024]{1,0:T(8,128)} fusion(bf16[16,512]{1,0:T(8,128)(2,1)S(1)} %reshape.171, bf16[2,512,1024]{2,1,0:T(8,128)(2,1)} %param.21), kind=kOutput, calls=%fused_computation.13 | convolution fusion | flops 16777216 | bytes 1130496 | tf_op jit(solution)/shard_map/dot_general | solution.py:50
  158.9 2.8 %pad_maximum_fusion = f32[2,4,8,64,64]{4,3,2,1,0:T(8,128)} fusion(f32[1,4,8,64,64]{4,3,2,1,0:T(8,128)} %get-tuple-element.13, f32[1,4,8,64,64]{4,3,2,1,0:T(8,128)S(1)} %get-tuple-element.12), kind=kLoop, calls=%fused_computation | loop fusion | flops 262144 | bytes 2097152 | tf_op jit(solution)/shard_map/stack | solution.py:94
  161.6 31.7 %all-reduce.9.cloned.1.call-done = f32[16,1024]{1,0:T(8,128)} async-done(((f32[16,1024]{1,0:T(8,128)}), f32[16,1024]{1,0:T(8,128)}) %all-reduce.9.cloned.1.call-update) | async-done | bytes 65552 | tf_op jit(solution)/shard_map/psum | solution.py:55
  193.3 1.5 fusion.65
  (64 shorter events, 3.4 us)
Async XLA Ops:
  7.2 4.1 %copy-start.1 = (bf16[16,1024]{1,0:T(8,128)(2,1)S(1)}, bf16[16,1024]{1,0:T(8,128)(2,1)}, u32[]{:S(2)}) copy-start(bf16[16,1024]{1,0:T(8,128)(2,1)} %param.12) | copy-start | bytes 98308
  7.2 4.1 %copy-start.2 = (bf16[2,1024,512]{2,1,0:T(8,128)(2,1)S(1)}, bf16[2,1024,512]{2,1,0:T(8,128)(2,1)}, u32[]{:S(2)}) copy-start(bf16[2,1024,512]{2,1,0:T(8,128)(2,1)} %param.17) | copy-start | bytes 6291460
  7.2 43.3 %all-reduce.11.cloned.1.call-start = ((), (), s32[]{:S(2)}) async-start(), calls=%async_computation.2 | async-start | bytes 393216
  8.1 5.0 %copy-start.4 = (bf16[2,1024,512]{2,1,0:T(8,128)(2,1)S(1)}, bf16[2,1024,512]{2,1,0:T(8,128)(2,1)}, u32[]{:S(2)}) copy-start(bf16[2,1024,512]{2,1,0:T(8,128)(2,1)} %param.19) | copy-start | bytes 6291460
  11.2 12.9 %copy-start.8 = (bf16[2,512]{1,0:T(2,128)(2,1)S(1)}, bf16[2,512]{1,0:T(2,128)(2,1)}, u32[]{:S(2)}) copy-start(bf16[2,512]{1,0:T(2,128)(2,1)} %param.23) | copy-start | bytes 6148
  11.2 12.9 %copy-start.9 = (f32[2,512]{1,0:T(2,128)S(1)}, f32[2,512]{1,0:T(2,128)}, u32[]{:S(2)}) copy-start(f32[2,512]{1,0:T(2,128)} %param.22) | copy-start | bytes 12292
  11.5 12.9 %copy-start.10 = (u32[32]{0:T(128)S(1)}, u32[32]{0:T(128)}, u32[]{:S(2)}) copy-start(u32[32]{0:T(128)} %constant.34) | copy-start | bytes 388
  11.5 40.2 %copy-start = (f32[2,4,8,64,64]{4,3,2,1,0:T(8,128)S(1)}, f32[2,4,8,64,64]{4,3,2,1,0:T(8,128)}, u32[]{:S(2)}) copy-start(f32[2,4,8,64,64]{4,3,2,1,0:T(8,128)} %param.13) | copy-start | bytes 3145732
  14.9 0.7 copy-start.6
  15.6 82.2 %all-reduce.7.cloned.1.call-start = ((), (), s32[]{:S(2)}) async-start(), calls=%async_computation | async-start | bytes 131072 | tf_op jit(solution)/shard_map/psum | solution.py:55
  63.3 80.5 %all-reduce.13.cloned.1.call-start = ((), (), s32[]{:S(2)}) async-start(), calls=%async_computation.3 | async-start | bytes 393216
  104.4 3.1 %copy-start.3 = (bf16[2,1024,512]{2,1,0:T(8,128)(2,1)S(1)}, bf16[2,1024,512]{2,1,0:T(8,128)(2,1)}, u32[]{:S(2)}) copy-start(bf16[2,1024,512]{2,1,0:T(8,128)(2,1)} %param.17) | copy-start | bytes 6291460
  104.4 4.8 %copy-start.5 = (bf16[2,1024,512]{2,1,0:T(8,128)(2,1)S(1)}, bf16[2,1024,512]{2,1,0:T(8,128)(2,1)}, u32[]{:S(2)}) copy-start(bf16[2,1024,512]{2,1,0:T(8,128)(2,1)} %param.19) | copy-start | bytes 6291460
  111.0 0.7 copy-start.7
  111.7 81.6 %all-reduce.9.cloned.1.call-start = ((), (), s32[]{:S(2)}) async-start(), calls=%async_computation.1 | async-start | bytes 131072 | tf_op jit(solution)/shard_map/psum | solution.py:55
Sparse Core Ops, SparseCore 0:
  15.7 34.7 all-reduce.10
  63.5 34.3 all-reduce.6
  111.8 31.9 all-reduce.12
  159.0 34.2 all-reduce.8
where the time goes:
time: 202 us; the launch traced here: 201 us
  waiting for transfers between devices  123 us (61%)
  matrix products  25.1 us (12%)
  blocking collectives  24.5 us (12%)
  between operations  14.5 us (7%)
  other arithmetic  11.5 us (6%)
  local copies, waits for them, and re-layouts  2.74 us (1%)
    psum x2, waiting for transfers between devices, run_block(): branch = lax.psum(branch_part, 'tp')  66 us
    unnamed x6, waiting for transfers between devices  56.8 us
    psum x2, blocking collectives, run_block(): all_totals = lax.psum(squares, 'dp')  14.1 us
    dot_general x12, matrix products, run_block(): jnp.dot(normed, weight, preferred_element_type=jnp.float32)  13.3 us
    all_gather x2, blocking collectives, run_block(): lax.all_gather(mixed, 'dp', axis=0, tiled=True)  10.4 us
    dot_general x2, matrix products, run_block(): jnp.dot(lax.all_gather(mixed, 'dp', axis=0, tiled=True), out_weight, pref...  4.2 us
    dot_general x2, matrix products, run_block(): jnp.einsum('bhij,bhj->bhi', new_state, recept, precision=lax.Precision.HI...  4.16 us
  transfers between devices with their start and end apart: 4, of which 4 were waited for; matrix products, arithmetic and copies ran while one was open for 2% of the time, Pallas kernels for 0%

commit v1 on v0

--- a/solution.py
+++ b/solution.py
@@ -52,7 +52,17 @@
         out_weight,
         preferred_element_type=jnp.float32,
     )
-    branch = lax.psum(branch_part, "tp")
+
+    def _carry_members_all(raw, chip_axis="tp"):
+        n = lax.axis_size(chip_axis)
+        plain = lambda inter: [(dev, dev ^ inter) for dev in range(n)]
+        u1 = raw
+        for rr in range(n.bit_length() - 1):
+            top = plain(1 << rr)
+            u1 = u1 + lax.ppermute(u1, chip_axis, top)
+        return u1
+
+    branch = _carry_members_all(branch_part)
     return ((current + branch).astype(jnp.bfloat16), new_state)
 
 

time: 202 us -> 148 us (0.73)
  waiting for transfers between devices: 123 us -> 65.9 us
  starting transfers between devices: 0.16 us -> 8 us
  other arithmetic: 11.5 us -> 7.82 us
    psum x2 -> x0, waiting for transfers between devices: 66 us -> none  [run_block(): branch = lax.psum(branch_part, 'tp')]
    ppermute x0 -> x4, waiting for transfers between devices: none -> 8.45 us  [_carry_members_all(): u1 = u1 + lax.ppermute(u1, chip_axis, top)]
    ppermute x0 -> x4, starting transfers between devices: none -> 7.92 us  [_carry_members_all(): u1 = u1 + lax.ppermute(u1, chip_axis, top)]
    unnamed x6 -> x4, waiting for transfers between devices: 56.8 us -> 57.5 us
  transfers between devices with their start and end apart: 4 -> 6, of which waited for: 4 -> 6; matrix products, arithmetic and copies ran while one was open for 2% -> 3% of each run, Pallas kernels for 0% -> 0%
where the time goes in v1:
time: 148 us
  waiting for transfers between devices  65.9 us (45%)
  blocking collectives  24.7 us (17%)
  matrix products  23.9 us (16%)
  between operations  14.8 us (10%)
  starting transfers between devices  8 us (5%)
  other arithmetic  7.82 us (5%)
  local copies, waits for them, and re-layouts  2.74 us (2%)
    unnamed x4, waiting for transfers between devices  57.5 us
    psum x2, blocking collectives, run_block(): all_totals = lax.psum(squares, 'dp')  14.3 us
    dot_general x12, matrix products, run_block(): jnp.dot(normed, weight, preferred_element_type=jnp.float32)  13.3 us
    all_gather x2, blocking collectives, run_block(): lax.all_gather(mixed, 'dp', axis=0, tiled=True)  10.4 us
    ppermute x4, waiting for transfers between devices, _carry_members_all(): u1 = u1 + lax.ppermute(u1, chip_axis, top)  8.45 us
    ppermute x4, starting transfers between devices, _carry_members_all(): u1 = u1 + lax.ppermute(u1, chip_axis, top)  7.92 us
    dot_general x2, matrix products, run_block(): jnp.einsum('bhij,bhj->bhi', new_state, recept, precision=lax.Precision.HI...  4.17 us
    dot_general x2, matrix products, run_block(): jnp.einsum('bhij,bhj->bhi', state_blk, unit_key, precision=lax.Precision....  3.49 us
  transfers between devices with their start and end apart: 6, of which 6 were waited for; matrix products, arithmetic and copies ran while one was open for 3% of the time, Pallas kernels for 0%

profile of v1, /device:TPU:0, one launch (start us, length us, event | category | flops | bytes accessed | tf_op | source)
XLA Modules:
  0.0 147.8 jit_solution(5149260639286493216)
XLA Ops:
  8.1 1.6 %convolution_dynamic-update-slice_fusion.11 = f32[16,3072]{1,0:T(8,128)S(1)} fusion(bf16[2,1024,512]{2,1,0:T(8,128)(2,1)} %param.15, bf16[16,1024]{1,0:T(8,128)(2,1)} %param.12, f32[1024]{0:T(1024)S(1)} %bitcast.173), kind=kOutput, calls=%fused_computation.12 | convolution fusion | flops 16826368 | bytes 1118208 | tf_op jit(solution)/shard_map/dot_general | solution.py:21
  9.7 1.5 %convolution_dynamic-update-slice_fusion.10 = f32[16,3072]{1,0:T(8,128)S(1)} fusion(f32[16,3072]{1,0:T(8,128)S(1)} %convolution_dynamic-update-slice_fusion.11, bf16[2,1024,512]{2,1,0:T(8,128)(2,1)} %param.16, bf16[16,1024]{1,0:T(8,128)(2,1)} %param.12, f32[1024]{0:T(1024)S(1)} %bitcast.174), kind=kOutput, calls=%fused_computation.11 | convolution fusion | flops 16826368 | bytes 1118208 | tf_op jit(solution)/shard_map/dot_general | solution.py:21
  11.5 1.6 %convolution_dynamic-update-slice_fusion.8 = f32[16,3072]{1,0:T(8,128)S(1)} fusion(f32[16,3072]{1,0:T(8,128)S(1)} %convolution_dynamic-update-slice_fusion.9, bf16[2,1024,512]{2,1,0:T(8,128)(2,1)} %param.18, bf16[16,1024]{1,0:T(8,128)(2,1)S(1)} %copy-done.1, f32[1024]{0:T(1024)S(1)} %bitcast.176), kind=kOutput, calls=%fused_computation.9 | convolution fusion | flops 16826368 | bytes 1118208 | tf_op jit(solution)/shard_map/dot_general | solution.py:21
  13.4 1.5 convolution_dynamic-update-slice_fusion.6
  15.8 8.4 %psum.14 = f32[16]{0:T(128)S(1)} all-reduce(f32[16]{0:T(128)S(1)} %fusion.61), channel_id=1, replica_groups=mesh['grp'=2,'tp'=4,'dp'=4] {'dp'}, use_global_device_ids=true, to_apply=%region_2.0 | all-reduce | flops 16 | bytes 128 | tf_op jit(solution)/shard_map/psum | solution.py:16
  25.7 24.8 %all-reduce.5.cloned.1.call-done = f32[16,3072]{1,0:T(8,128)} async-done(((f32[16,3072]{1,0:T(8,128)}), f32[16,3072]{1,0:T(8,128)}) %all-reduce.5.cloned.1.call-update) | async-done | bytes 196624
  50.5 1.0 dynamic-slice_multiply_fusion.1
  51.7 1.7 %fusion.22 = f32[4,8,1,64]{3,2,1,0:T(1,128)S(1)} fusion(f32[4,8,64,1]{2,3,1,0:T(1,128)S(1)} %bitcast.189, f32[2,4,8,64,64]{4,3,2,1,0:T(8,128)S(1)} %copy-done), kind=kOutput, calls=%fused_computation.35 | convolution fusion | flops 1572864 | bytes 1073152 | tf_op jit(solution)/shard_map/bhij,bhj->bhi/dot_general | solution.py:39
  53.5 2.1 %fusion.26 = f32[4,8,1,64]{3,2,1,0:T(1,128)S(1)} fusion(f32[4,8,64,1]{2,3,1,0:T(1,128)S(1)} %bitcast.191, f32[2,4,8,64,64]{4,3,2,1,0:T(8,128)S(1)} %copy-done, f32[4,8,64]{2,1,0:T(8,128)S(1)} %get-tuple-element.23, f32[4,8,64]{2,1,0:T(8,128)S(1)} %get-tuple-element.21, f32[4,8,64]{2,1,0:T(8,128)S(1)} %get-tuple-element.10, f32[4,8,64]{2,1,0:T(8,128)S(1)} %bitcast.185, ...), kind=kOutput, calls=%fused_computation.40 | convolution fusion | flops 2228224 | bytes 1155072 | tf_op jit(solution)/shard_map/bhij,bhj->bhi/dot_general | solution.py:45
  56.0 5.2 %all-gather = bf16[4,4,512]{2,1,0:T(4,128)(2,1)S(1)} all-gather(bf16[1,4,512]{2,1,0:T(4,128)(2,1)S(1)} %reshape.168), channel_id=1, replica_groups=mesh['grp'=2,'tp'=4,'dp'=4] {'dp'}, dimensions={0}, use_global_device_ids=true | all-gather | bytes 20480 | tf_op jit(solution)/shard_map/all_gather | solution.py:51
  61.2 1.5 fusion.14
  62.7 1.5 %collective-permute-start = (f32[16,1024]{1,0:T(8,128)S(1)}, f32[16,1024]{1,0:T(8,128)S(1)}, u32[]{:S(2)}, u32[]{:S(2)}) collective-permute-start(f32[16,1024]{1,0:T(8,128)S(1)} %fusion.14), channel_id=1, source_target_pairs={{0,4},{4,0},{8,12},{12,8},{1,5},{5,1},{9,13},{13,9},{2,6},{6,2},{1... | collective-permute-start | bytes 196616 | tf_op jit(solution)/shard_map/ppermute | solution.py:62
  64.2 2.9 %collective-permute-done = f32[16,1024]{1,0:T(8,128)S(1)} collective-permute-done((f32[16,1024]{1,0:T(8,128)S(1)}, f32[16,1024]{1,0:T(8,128)S(1)}, u32[]{:S(2)}, u32[]{:S(2)}) %collective-permute-start) | collective-permute-done | bytes 65568 | tf_op jit(solution)/shard_map/ppermute | solution.py:62
  67.0 2.5 %collective-permute-start.1 = (f32[16,1024]{1,0:T(8,128)S(1)}, f32[16,1024]{1,0:T(8,128)S(1)}, u32[]{:S(2)}, u32[]{:S(2)}) collective-permute-start(f32[16,1024]{1,0:T(8,128)S(1)} %add.157), channel_id=1, source_target_pairs={{0,8},{4,12},{8,0},{12,4},{1,9},{5,13},{9,1},{13,5},{2,10},{6,14},... | collective-permute-start | bytes 196616 | tf_op jit(solution)/shard_map/ppermute | solution.py:62
  69.7 2.7 %collective-permute-done.1 = f32[16,1024]{1,0:T(8,128)S(1)} collective-permute-done((f32[16,1024]{1,0:T(8,128)S(1)}, f32[16,1024]{1,0:T(8,128)S(1)}, u32[]{:S(2)}, u32[]{:S(2)}) %collective-permute-start.1) | collective-permute-done | bytes 65568 | tf_op jit(solution)/shard_map/ppermute | solution.py:62
  72.5 5.9 %psum.15 = f32[16]{0:T(128)S(1)} all-reduce(f32[16]{0:T(128)S(1)} %get-tuple-element.8), channel_id=1, replica_groups=mesh['grp'=2,'tp'=4,'dp'=4] {'dp'}, use_global_device_ids=true, to_apply=%region_8.0 | all-reduce | flops 16 | bytes 128 | tf_op jit(solution)/shard_map/psum | solution.py:16
  78.4 1.6 %convolution_dynamic-update-slice_fusion.5 = f32[16,3072]{1,0:T(8,128)S(1)} fusion(bf16[2,1024,512]{2,1,0:T(8,128)(2,1)} %param.15, bf16[16,1024]{1,0:T(8,128)(2,1)S(1)} %get-tuple-element.9, f32[1024]{0:T(1024)S(1)} %bitcast.167), kind=kOutput, calls=%fused_computation.6 | convolution fusion | flops 16826368 | bytes 1118208 | tf_op jit(solution)/shard_map/dot_general | solution.py:21
  80.0 1.5 convolution_dynamic-update-slice_fusion.4
  81.8 1.5 convolution_dynamic-update-slice_fusion.2
  83.5 1.5 convolution_dynamic-update-slice_fusion
  85.8 32.6 %all-reduce.7.cloned.1.call-done = f32[16,3072]{1,0:T(8,128)} async-done(((f32[16,3072]{1,0:T(8,128)}), f32[16,3072]{1,0:T(8,128)}) %all-reduce.7.cloned.1.call-update) | async-done | bytes 196624
  118.4 1.0 dynamic-slice_multiply_fusion
  119.7 1.7 %fusion.8 = f32[4,8,1,64]{3,2,1,0:T(1,128)S(1)} fusion(f32[4,8,64,1]{2,3,1,0:T(1,128)S(1)} %bitcast.190, f32[2,4,8,64,64]{4,3,2,1,0:T(8,128)S(1)} %copy-done), kind=kOutput, calls=%fused_computation.21 | convolution fusion | flops 1572864 | bytes 1073152 | tf_op jit(solution)/shard_map/bhij,bhj->bhi/dot_general | solution.py:39
  121.4 2.1 %fusion.12 = f32[4,8,1,64]{3,2,1,0:T(1,128)S(1)} fusion(f32[4,8,64,1]{2,3,1,0:T(1,128)S(1)} %bitcast.192, f32[2,4,8,64,64]{4,3,2,1,0:T(8,128)S(1)} %copy-done, f32[4,8,64]{2,1,0:T(8,128)S(1)} %get-tuple-element.18, f32[4,8,64]{2,1,0:T(8,128)S(1)} %get-tuple-element.16, f32[4,8,64]{2,1,0:T(8,128)S(1)} %get-tuple-element.6, f32[4,8,64]{2,1,0:T(8,128)S(1)} %bitcast.187, ...), kind=kOutput, calls=%fused_computation.26 | convolution fusion | flops 2228224 | bytes 1155072 | tf_op jit(solution)/shard_map/bhij,bhj->bhi/dot_general | solution.py:45
  123.9 5.2 %all-gather.1 = bf16[4,4,512]{2,1,0:T(4,128)(2,1)S(1)} all-gather(bf16[1,4,512]{2,1,0:T(4,128)(2,1)S(1)} %reshape.170), channel_id=1, replica_groups=mesh['grp'=2,'tp'=4,'dp'=4] {'dp'}, dimensions={0}, use_global_device_ids=true | all-gather | bytes 20480 | tf_op jit(solution)/shard_map/all_gather | solution.py:51
  129.1 1.5 fusion
  130.6 1.5 %collective-permute-start.2 = (f32[16,1024]{1,0:T(8,128)S(1)}, f32[16,1024]{1,0:T(8,128)S(1)}, u32[]{:S(2)}, u32[]{:S(2)}) collective-permute-start(f32[16,1024]{1,0:T(8,128)S(1)} %fusion), channel_id=1, source_target_pairs={{0,4},{4,0},{8,12},{12,8},{1,5},{5,1},{9,13},{13,9},{2,6},{6,2},{1... | collective-permute-start | bytes 196616 | tf_op jit(solution)/shard_map/ppermute | solution.py:62
  132.1 1.4 multiply_add_fusion.1
  133.5 1.4 collective-permute-done.2
  135.0 2.5 %collective-permute-start.3 = (f32[16,1024]{1,0:T(8,128)S(1)}, f32[16,1024]{1,0:T(8,128)S(1)}, u32[]{:S(2)}, u32[]{:S(2)}) collective-permute-start(f32[16,1024]{1,0:T(8,128)S(1)} %add.170), channel_id=1, source_target_pairs={{0,8},{4,12},{8,0},{12,4},{1,9},{5,13},{9,1},{13,5},{2,10},{6,14},... | collective-permute-start | bytes 196616 | tf_op jit(solution)/shard_map/ppermute | solution.py:62
  137.5 1.5 %pad_maximum_fusion = f32[2,4,8,64,64]{4,3,2,1,0:T(8,128)} fusion(f32[1,4,8,64,64]{4,3,2,1,0:T(8,128)S(1)} %get-tuple-element.13, f32[1,4,8,64,64]{4,3,2,1,0:T(8,128)S(1)} %get-tuple-element.12), kind=kLoop, calls=%fused_computation | loop fusion | flops 262144 | bytes 2097152 | tf_op jit(solution)/shard_map/stack | solution.py:104
  138.9 1.4 collective-permute-done.3
  (68 shorter events, 6.8 us)
Async XLA Ops:
  7.2 4.1 %copy-start.1 = (bf16[16,1024]{1,0:T(8,128)(2,1)S(1)}, bf16[16,1024]{1,0:T(8,128)(2,1)}, u32[]{:S(2)}) copy-start(bf16[16,1024]{1,0:T(8,128)(2,1)} %param.12) | copy-start | bytes 98308
  7.2 4.1 %copy-start.2 = (bf16[2,1024,512]{2,1,0:T(8,128)(2,1)S(1)}, bf16[2,1024,512]{2,1,0:T(8,128)(2,1)}, u32[]{:S(2)}) copy-start(bf16[2,1024,512]{2,1,0:T(8,128)(2,1)} %param.17) | copy-start | bytes 6291460
  7.2 43.3 %all-reduce.5.cloned.1.call-start = ((), (), s32[]{:S(2)}) async-start(), calls=%async_computation | async-start | bytes 393216
  8.1 5.0 %copy-start.4 = (bf16[2,1024,512]{2,1,0:T(8,128)(2,1)S(1)}, bf16[2,1024,512]{2,1,0:T(8,128)(2,1)}, u32[]{:S(2)}) copy-start(bf16[2,1024,512]{2,1,0:T(8,128)(2,1)} %param.19) | copy-start | bytes 6291460
  11.2 12.9 %copy-start.8 = (bf16[2,512]{1,0:T(2,128)(2,1)S(1)}, bf16[2,512]{1,0:T(2,128)(2,1)}, u32[]{:S(2)}) copy-start(bf16[2,512]{1,0:T(2,128)(2,1)} %param.23) | copy-start | bytes 6148
  11.2 12.9 %copy-start.9 = (f32[2,512]{1,0:T(2,128)S(1)}, f32[2,512]{1,0:T(2,128)}, u32[]{:S(2)}) copy-start(f32[2,512]{1,0:T(2,128)} %param.22) | copy-start | bytes 12292
  11.5 12.9 %copy-start.10 = (u32[32]{0:T(128)S(1)}, u32[32]{0:T(128)}, u32[]{:S(2)}) copy-start(u32[32]{0:T(128)} %constant.34) | copy-start | bytes 388
  11.5 40.2 %copy-start = (f32[2,4,8,64,64]{4,3,2,1,0:T(8,128)S(1)}, f32[2,4,8,64,64]{4,3,2,1,0:T(8,128)}, u32[]{:S(2)}) copy-start(f32[2,4,8,64,64]{4,3,2,1,0:T(8,128)} %param.13) | copy-start | bytes 3145732
  14.9 0.7 copy-start.6
  15.6 102.8 %all-reduce.7.cloned.1.call-start = ((), (), s32[]{:S(2)}) async-start(), calls=%async_computation.1 | async-start | bytes 393216
  62.7 4.3 %collective-permute-start = (f32[16,1024]{1,0:T(8,128)S(1)}, f32[16,1024]{1,0:T(8,128)S(1)}, u32[]{:S(2)}, u32[]{:S(2)}) collective-permute-start(f32[16,1024]{1,0:T(8,128)S(1)} %fusion.14), channel_id=1, source_target_pairs={{0,4},{4,0},{8,12},{12,8},{1,5},{5,1},{9,13},{13,9},{2,6},{6,2},{1... | collective-permute-start | bytes 196616 | tf_op jit(solution)/shard_map/ppermute | solution.py:62
  67.0 5.4 %collective-permute-start.1 = (f32[16,1024]{1,0:T(8,128)S(1)}, f32[16,1024]{1,0:T(8,128)S(1)}, u32[]{:S(2)}, u32[]{:S(2)}) collective-permute-start(f32[16,1024]{1,0:T(8,128)S(1)} %add.157), channel_id=1, source_target_pairs={{0,8},{4,12},{8,0},{12,4},{1,9},{5,13},{9,1},{13,5},{2,10},{6,14},... | collective-permute-start | bytes 196616 | tf_op jit(solution)/shard_map/ppermute | solution.py:62
  78.4 3.1 %copy-start.3 = (bf16[2,1024,512]{2,1,0:T(8,128)(2,1)S(1)}, bf16[2,1024,512]{2,1,0:T(8,128)(2,1)}, u32[]{:S(2)}) copy-start(bf16[2,1024,512]{2,1,0:T(8,128)(2,1)} %param.17) | copy-start | bytes 6291460
  78.4 4.8 %copy-start.5 = (bf16[2,1024,512]{2,1,0:T(8,128)(2,1)S(1)}, bf16[2,1024,512]{2,1,0:T(8,128)(2,1)}, u32[]{:S(2)}) copy-start(bf16[2,1024,512]{2,1,0:T(8,128)(2,1)} %param.19) | copy-start | bytes 6291460
  85.0 0.7 copy-start.7
  130.6 4.3 %collective-permute-start.2 = (f32[16,1024]{1,0:T(8,128)S(1)}, f32[16,1024]{1,0:T(8,128)S(1)}, u32[]{:S(2)}, u32[]{:S(2)}) collective-permute-start(f32[16,1024]{1,0:T(8,128)S(1)} %fusion), channel_id=1, source_target_pairs={{0,4},{4,0},{8,12},{12,8},{1,5},{5,1},{9,13},{13,9},{2,6},{6,2},{1... | collective-permute-start | bytes 196616 | tf_op jit(solution)/shard_map/ppermute | solution.py:62
  135.0 5.4 %collective-permute-start.3 = (f32[16,1024]{1,0:T(8,128)S(1)}, f32[16,1024]{1,0:T(8,128)S(1)}, u32[]{:S(2)}, u32[]{:S(2)}) collective-permute-start(f32[16,1024]{1,0:T(8,128)S(1)} %add.170), channel_id=1, source_target_pairs={{0,8},{4,12},{8,0},{12,4},{1,9},{5,13},{9,1},{13,5},{2,10},{6,14},... | collective-permute-start | bytes 196616 | tf_op jit(solution)/shard_map/ppermute | solution.py:62
Sparse Core Ops, SparseCore 0:
  15.7 34.7 all-reduce.4
  85.8 32.5 all-reduce.6
